TPU v7x, 256 devices: a 4x2x16 block of a 4x16x16 slice. The times are simulated.
256 devices in a mesh: grp: 2 (over y), sp: 32 (over z, core), tp: 4 (over x).
Axes of the slice: x: 4, y: 2, z: 16, core: 2. Of those that a mesh axis runs over, the one named last changes fastest.
The devices are a block of a 4x16x16 slice.
Arguments:
- stream: bfloat16 [16384, 4096], P(('grp', 'sp'), 'tp'), parts along dimension 0, may hold values from -6 to 6
- gain_pre: float32 [3, 4096], replicated, may hold values from 0.1 to 1.9
- w_in: bfloat16 [3, 4096, 1024], P(None, 'sp', 'tp'), may hold values from -0.09375 to 0.09375
- w_pool: bfloat16 [3, 4, 256, 256], P(None, 'tp'), may hold values from -0.375 to 0.375
- pool_scale: float32 [3, 1024], P(None, 'tp'), may hold values from 0.1 to 1.9
- w_out: bfloat16 [3, 1024, 4096], P(None, 'tp', 'sp'), may hold values from -0.5 to 0.5
- gain_post: float32 [3, 4096], replicated, may hold values from 0.1 to 1.9
Outputs:
- result: bfloat16 [16384, 4096], P(('grp', 'sp'), 'tp'), parts along dimension 0
There are 2 independent parts, one for each index of `grp`. A program takes and returns all parts, laid end to end along the dimension named above; an argument that names none is the same for every part. Nothing has to cross between parts.
All inputs are finite; a program needn't handle non-finite values.
Results may differ from a plain program's by a relative error of at most 0.02.
Values may be sent and summed in bfloat16 or wider, within the bound.
A program may use at most 64 MiB of HBM per device.

v0:
```python
import jax
import jax.numpy as jnp
from jax import lax
from jax.sharding import PartitionSpec as P

LAYERS = 3


WINDOWS = (2, 4, 8, 16)
EPS = 1e-06


def rows_first(arrays, axis, dims):
    turned = [jnp.moveaxis(a, dim, 0) for a, dim in zip(arrays, dims)]
    widths = [t[0].size for t in turned]
    both = jnp.concatenate([t.reshape(-1, w) for t, w in zip(turned, widths)], axis=1)
    result = lax.all_gather(both, axis, axis=0, tiled=True)
    tiles = jnp.split(result, [sum(widths[:k]) for k in range(1, len(widths))], axis=1)
    return tuple(
        (
            jnp.moveaxis(b.reshape(-1, *t.shape[1:]), 0, dim)
            for b, t, dim in zip(tiles, turned, dims)
        )
    )


def from_behind(block, axis, distance):
    devices = range(lax.axis_size(axis))
    route = [(i - distance, i) for i in devices if i - distance in devices]
    return lax.ppermute(block, axis, route)


def copy_for_each(array, axis):
    copies = jnp.broadcast_to(array, (lax.axis_size(axis), *array.shape))
    return lax.all_to_all(copies, axis, split_axis=0, concat_axis=0, tiled=True)


def joined_along(tiles, dim):
    tiles = jnp.moveaxis(tiles, 0, dim)
    dims = tiles.shape
    return tiles.reshape(*dims[:dim], dims[dim] * dims[dim + 1], *dims[dim + 2 :])


def gather_directly(array, axis, dim):
    tiles = copy_for_each(array, axis)
    return joined_along(tiles, dim)


def in_blocks(array, dim, size):
    before, after = (array.shape[:dim], array.shape[dim + 1 :])
    return jnp.moveaxis(array.reshape(*before, size, -1, *after), dim, 0)


def sent_and_summed(array, axis, dim):
    size = lax.axis_size(axis)
    tiles = lax.all_to_all(in_blocks(array, dim, size), axis, 0, 0, tiled=True)
    return jnp.sum(tiles.astype(jnp.float32), axis=0)


def taken_together(array, axis):
    everything = copy_for_each(array, axis)
    return jnp.sum(everything, axis=0)


def rms_scale(values, gain):
    inverse = lax.rsqrt(jnp.mean(values * values, axis=-1, keepdims=True) + EPS)
    return values * inverse * gain[None, :]


def per_device(stream, gain_pre, w_in, w_pool, pool_scale, w_out, gain_post):
    tok_rows = stream.shape[0]
    block_width = stream.shape[1]
    width = gain_pre.shape[1]
    group = w_pool.shape[2]
    reach = max(WINDOWS) - 1
    group_index = lax.axis_index("tp")
    window = jnp.where(
        group_index == 0, 2, jnp.where(group_index == 1, 4, jnp.where(group_index == 2, 8, 16))
    )
    positions = lax.axis_index("sp") * tok_rows + lax.iota(jnp.int32, tok_rows)
    count = jnp.minimum(positions + 1, window).astype(jnp.float32)
    gathered_in, gathered_out = rows_first((w_in, w_out), "sp", (1, 2))
    current = stream
    feature_start = group_index * block_width
    for layer in range(LAYERS):
        full_rows = gather_directly(current, "tp", 1)
        normed = rms_scale(full_rows.astype(jnp.float32), gain_pre[layer]).astype(jnp.bfloat16)
        inner_sum = jnp.dot(normed, gathered_in[layer], preferred_element_type=jnp.float32)
        inner = inner_sum.astype(jnp.bfloat16)
        rim = from_behind(inner[tok_rows - reach :], "sp", 1)
        extended = jnp.concatenate([rim, inner], axis=0).astype(jnp.float32)
        summed = jnp.zeros((tok_rows, group), jnp.float32)
        for offset in range(max(WINDOWS)):
            window_slice = extended[reach - offset : reach - offset + tok_rows]
            summed = summed + jnp.where(offset < window, window_slice, 0.0)
        pooled = summed / count[:, None]
        spread = (pooled - inner.astype(jnp.float32)).astype(jnp.bfloat16)
        mixed = jnp.dot(spread, w_pool[layer, 0], preferred_element_type=jnp.float32)
        mixed = (mixed * pool_scale[layer][None, :]).astype(jnp.bfloat16)
        partial_value = jnp.dot(mixed, gathered_out[layer], preferred_element_type=jnp.float32)
        partial_value = partial_value.astype(jnp.bfloat16)
        branch = sent_and_summed(partial_value, "tp", 1)
        squares = taken_together(jnp.sum(branch * branch, axis=1), "tp")
        inverse = lax.rsqrt(squares / width + EPS)
        gain_block = lax.dynamic_slice_in_dim(gain_post[layer], feature_start, block_width, 0)
        normed_branch = branch * inverse[:, None] * gain_block[None, :]
        current = (current.astype(jnp.float32) + normed_branch).astype(jnp.bfloat16)
    return current


def solution(mesh):
    return jax.shard_map(
        per_device,
        mesh=mesh,
        in_specs=(
            P(("grp", "sp"), "tp"),
            P(),
            P(None, "sp", "tp"),
            P(None, "tp", None, None),
            P(None, "tp"),
            P(None, "tp", "sp"),
            P(),
        ),
        out_specs=P(("grp", "sp"), "tp"),
        check_vma=False,
    )
```

profile of v0, /device:TPU:40, one launch (start us, length us, event | category | flops | bytes accessed | tf_op | source)
XLA Modules:
  0.0 363.0 jit_solution(6693995348859287650)
XLA Ops:
  6.6 1.1 copy.27
  7.6 1.7 pad_maximum_fusion
  9.4 1.2 copy.26
  10.7 1.5 broadcast_in_dim.81
  12.2 4.7 %all-to-all-start = ((bf16[4,256,1024]{1,2,0:T(8,128)(2,1)}), bf16[4,256,1024]{1,2,0:T(8,128)(2,1)S(1)}, u32[]{:S(2)}, u32[]{:S(2)}) async-start(bf16[4,256,1024]{1,2,0:T(8,128)(2,1)} %broadcast_in_dim.81), calls=%async_computation | async-start | bytes 4194304 | tf_op jit(solution)/shard_map/all_to_all | solution.py:35
  17.1 26.2 %all-to-all-done = bf16[4,256,1024]{1,2,0:T(8,128)(2,1)S(1)} async-done(((bf16[4,256,1024]{1,2,0:T(8,128)(2,1)}), bf16[4,256,1024]{1,2,0:T(8,128)(2,1)S(1)}, u32[]{:S(2)}, u32[]{:S(2)}) %all-to-all-start) | async-done | bytes 2097184 | tf_op jit(solution)/shard_map/all_to_all | solution.py:35
  43.3 0.6 fusion
  43.8 1.7 fusion.2
  45.5 91.5 %all-gather.2.cloned.1.call-done = bf16[4096,1536]{0,1:T(8,128)(2,1)} async-done(((bf16[128,1536]{0,1:T(8,128)(2,1)}), bf16[4096,1536]{0,1:T(8,128)(2,1)}) %all-gather.2.cloned.1.call-update) | async-done | bytes 12582928 | tf_op jit(solution)/shard_map/all_gather | solution.py:17
  137.0 8.4 %fusion.207 = (bf16[4096,768]{0,1:T(8,128)(2,1)S(1)}, bf16[4096,768]{0,1:T(8,128)(2,1)}) fusion(bf16[4096,1536]{0,1:T(8,128)(2,1)} %all-gather.2.cloned.1.call-done), kind=kLoop, calls=%fused_computation.233 | loop fusion | bytes 25165824 | tf_op jit(solution)/shard_map/split | solution.py:18
  145.4 2.7 copy-done
  148.1 0.8 fusion.15
  148.9 2.2 collective-permute-start
  151.1 0.8 collective-permute-done
  151.9 3.0 convolution_convert_fusion.2
  154.9 1.6 copy.47
  156.5 4.4 %all-to-all-start.1 = ((bf16[4,256,1024]{2,1,0:T(8,128)(2,1)}), bf16[4,256,1024]{2,1,0:T(8,128)(2,1)S(1)}, u32[]{:S(2)}, u32[]{:S(2)}) async-start(bf16[4,256,1024]{2,1,0:T(8,128)(2,1)} %bitcast.87), calls=%async_computation.1 | async-start | bytes 4194304 | tf_op jit(solution)/shard_map/all_to_all | solution.py:56
  161.0 26.8 %all-to-all-done.1 = bf16[4,256,1024]{2,1,0:T(8,128)(2,1)S(1)} async-done(((bf16[4,256,1024]{2,1,0:T(8,128)(2,1)}), bf16[4,256,1024]{2,1,0:T(8,128)(2,1)S(1)}, u32[]{:S(2)}, u32[]{:S(2)}) %all-to-all-start.1) | async-done | bytes 2097184 | tf_op jit(solution)/shard_map/all_to_all | solution.py:56
  188.3 0.6 broadcast_in_dim.83
  188.9 3.3 all-to-all-start.2
  192.2 5.2 %all-to-all-done.2 = f32[4,1,256]{2,1,0:T(1,128)S(1)} async-done(((f32[4,1,256]{2,1,0:T(1,128)}), f32[4,1,256]{2,1,0:T(1,128)S(1)}, u32[]{:S(2)}, u32[]{:S(2)}) %all-to-all-start.2) | async-done | bytes 4128 | tf_op jit(solution)/shard_map/all_to_all | solution.py:35
  197.5 1.3 add_convert_fusion.2
  198.9 1.5 broadcast_in_dim.84
  200.4 3.7 %all-to-all-start.3 = ((bf16[4,256,1024]{1,2,0:T(8,128)(2,1)}), bf16[4,256,1024]{1,2,0:T(8,128)(2,1)S(1)}, u32[]{:S(2)}, u32[]{:S(2)}) async-start(bf16[4,256,1024]{1,2,0:T(8,128)(2,1)} %broadcast_in_dim.84), calls=%async_computation.3 | async-start | bytes 4194304 | tf_op jit(solution)/shard_map/all_to_all | solution.py:35
  204.1 24.7 %all-to-all-done.3 = bf16[4,256,1024]{1,2,0:T(8,128)(2,1)S(1)} async-done(((bf16[4,256,1024]{1,2,0:T(8,128)(2,1)}), bf16[4,256,1024]{1,2,0:T(8,128)(2,1)S(1)}, u32[]{:S(2)}, u32[]{:S(2)}) %all-to-all-start.3) | async-done | bytes 2097184 | tf_op jit(solution)/shard_map/all_to_all | solution.py:35
  228.8 0.6 fusion.3
  229.4 0.7 fusion.5
  230.2 2.4 fusion.16
  232.5 1.3 collective-permute-start.1
  233.9 0.8 collective-permute-done.1
  234.7 3.0 convolution_convert_fusion.1
  237.9 29.6 %all_to_all.48 = bf16[4,256,1024]{2,1,0:T(8,128)(2,1)S(1)} all-to-all(bf16[4,256,1024]{2,1,0:T(8,128)(2,1)S(1)} %bitcast.88), channel_id=1, replica_groups=mesh['grp'=2,'sp'=32,'tp'=4] {'tp'}, dimensions={0} | all-to-all | bytes 4194304 | tf_op jit(solution)/shard_map/all_to_all | solution.py:56
  268.1 0.6 broadcast_in_dim.85
  268.7 3.3 all-to-all-start.5
  272.0 5.2 %all-to-all-done.5 = f32[4,1,256]{2,1,0:T(1,128)S(1)} async-done(((f32[4,1,256]{2,1,0:T(1,128)}), f32[4,1,256]{2,1,0:T(1,128)S(1)}, u32[]{:S(2)}, u32[]{:S(2)}) %all-to-all-start.5) | async-done | bytes 4128 | tf_op jit(solution)/shard_map/all_to_all | solution.py:35
  277.7 1.5 broadcast_in_dim.86
  279.2 3.9 %all-to-all-start.6 = ((bf16[4,256,1024]{1,2,0:T(8,128)(2,1)}), bf16[4,256,1024]{1,2,0:T(8,128)(2,1)S(1)}, u32[]{:S(2)}, u32[]{:S(2)}) async-start(bf16[4,256,1024]{1,2,0:T(8,128)(2,1)} %broadcast_in_dim.86), calls=%async_computation.6 | async-start | bytes 4194304 | tf_op jit(solution)/shard_map/all_to_all | solution.py:35
  283.1 24.7 %all-to-all-done.6 = bf16[4,256,1024]{1,2,0:T(8,128)(2,1)S(1)} async-done(((bf16[4,256,1024]{1,2,0:T(8,128)(2,1)}), bf16[4,256,1024]{1,2,0:T(8,128)(2,1)S(1)}, u32[]{:S(2)}, u32[]{:S(2)}) %all-to-all-start.6) | async-done | bytes 2097184 | tf_op jit(solution)/shard_map/all_to_all | solution.py:35
  308.3 0.7 fusion.8
  309.0 2.4 fusion.17
  311.4 1.3 collective-permute-start.2
  312.8 0.8 collective-permute-done.2
  313.6 3.0 convolution_convert_fusion
  316.8 28.6 %all_to_all.49 = bf16[4,256,1024]{2,1,0:T(8,128)(2,1)S(1)} all-to-all(bf16[4,256,1024]{2,1,0:T(8,128)(2,1)S(1)} %bitcast.89), channel_id=1, replica_groups=mesh['grp'=2,'sp'=32,'tp'=4] {'tp'}, dimensions={0} | all-to-all | bytes 4194304 | tf_op jit(solution)/shard_map/all_to_all | solution.py:56
  345.9 0.6 broadcast_in_dim.87
  346.5 3.3 all-to-all-start.8
  349.9 5.2 %all-to-all-done.8 = f32[4,1,256]{2,1,0:T(1,128)S(1)} async-done(((f32[4,1,256]{2,1,0:T(1,128)}), f32[4,1,256]{2,1,0:T(1,128)S(1)}, u32[]{:S(2)}, u32[]{:S(2)}) %all-to-all-start.8) | async-done | bytes 4128 | tf_op jit(solution)/shard_map/all_to_all | solution.py:35
  355.1 1.0 add_convert_fusion
  (48 shorter events, 3.7 us)
Async XLA Ops:
  6.5 130.4 %all-gather.2.cloned.1.call-start = ((), (), s32[]{:S(2)}) async-start(), calls=%async_computation.9 | async-start | bytes 12976128 | tf_op jit(solution)/shard_map/all_gather | solution.py:17
  12.2 4.7 %copy-start.2 = (f32[3,4096]{1,0:T(4,128)S(1)}, f32[3,4096]{1,0:T(4,128)}, u32[]{:S(2)}) copy-start(f32[3,4096]{1,0:T(4,128)} %param.8) | copy-start | bytes 147460
  12.2 4.9 %copy-start.4 = (f32[3,256]{1,0:T(4,128)S(1)}, f32[3,256]{1,0:T(4,128)}, u32[]{:S(2)}) copy-start(f32[3,256]{1,0:T(4,128)} %param.11) | copy-start | bytes 9220
  12.2 31.1 %all-to-all-start = ((bf16[4,256,1024]{1,2,0:T(8,128)(2,1)}), bf16[4,256,1024]{1,2,0:T(8,128)(2,1)S(1)}, u32[]{:S(2)}, u32[]{:S(2)}) async-start(bf16[4,256,1024]{1,2,0:T(8,128)(2,1)} %broadcast_in_dim.81), calls=%async_computation | async-start | bytes 4194304 | tf_op jit(solution)/shard_map/all_to_all | solution.py:35
  45.5 102.6 %copy-start.1 = (bf16[4,256,1024]{1,2,0:T(8,128)(2,1)S(1)}, bf16[4,256,1024]{1,2,0:T(8,128)(2,1)}, u32[]{:S(2)}) copy-start(bf16[4,256,1024]{1,2,0:T(8,128)(2,1)} %fusion.2) | copy-start | bytes 6291460
  145.4 2.7 copy-start
  148.9 3.0 collective-permute-start
  156.5 4.4 %copy-start.3 = (f32[3,4096]{1,0:T(4,128)S(1)}, f32[3,4096]{1,0:T(4,128)}, u32[]{:S(2)}) copy-start(f32[3,4096]{1,0:T(4,128)} %param.13) | copy-start | bytes 147460
  156.5 31.2 %all-to-all-start.1 = ((bf16[4,256,1024]{2,1,0:T(8,128)(2,1)}), bf16[4,256,1024]{2,1,0:T(8,128)(2,1)S(1)}, u32[]{:S(2)}, u32[]{:S(2)}) async-start(bf16[4,256,1024]{2,1,0:T(8,128)(2,1)} %bitcast.87), calls=%async_computation.1 | async-start | bytes 4194304 | tf_op jit(solution)/shard_map/all_to_all | solution.py:56
  188.9 8.5 %all-to-all-start.2 = ((f32[4,1,256]{2,1,0:T(1,128)}), f32[4,1,256]{2,1,0:T(1,128)S(1)}, u32[]{:S(2)}, u32[]{:S(2)}) async-start(f32[4,1,256]{2,1,0:T(1,128)} %broadcast_in_dim.83), calls=%async_computation.2 | async-start | bytes 8192 | tf_op jit(solution)/shard_map/all_to_all | solution.py:35
  200.4 28.4 %all-to-all-start.3 = ((bf16[4,256,1024]{1,2,0:T(8,128)(2,1)}), bf16[4,256,1024]{1,2,0:T(8,128)(2,1)S(1)}, u32[]{:S(2)}, u32[]{:S(2)}) async-start(bf16[4,256,1024]{1,2,0:T(8,128)(2,1)} %broadcast_in_dim.84), calls=%async_computation.3 | async-start | bytes 4194304 | tf_op jit(solution)/shard_map/all_to_all | solution.py:35
  232.5 2.1 collective-permute-start.1
  268.7 8.5 %all-to-all-start.5 = ((f32[4,1,256]{2,1,0:T(1,128)}), f32[4,1,256]{2,1,0:T(1,128)S(1)}, u32[]{:S(2)}, u32[]{:S(2)}) async-start(f32[4,1,256]{2,1,0:T(1,128)} %broadcast_in_dim.85), calls=%async_computation.5 | async-start | bytes 8192 | tf_op jit(solution)/shard_map/all_to_all | solution.py:35
  279.2 28.6 %all-to-all-start.6 = ((bf16[4,256,1024]{1,2,0:T(8,128)(2,1)}), bf16[4,256,1024]{1,2,0:T(8,128)(2,1)S(1)}, u32[]{:S(2)}, u32[]{:S(2)}) async-start(bf16[4,256,1024]{1,2,0:T(8,128)(2,1)} %broadcast_in_dim.86), calls=%async_computation.6 | async-start | bytes 4194304 | tf_op jit(solution)/shard_map/all_to_all | solution.py:35
  311.4 2.1 collective-permute-start.2
  346.5 8.5 %all-to-all-start.8 = ((f32[4,1,256]{2,1,0:T(1,128)}), f32[4,1,256]{2,1,0:T(1,128)S(1)}, u32[]{:S(2)}, u32[]{:S(2)}) async-start(f32[4,1,256]{2,1,0:T(1,128)} %broadcast_in_dim.87), calls=%async_computation.8 | async-start | bytes 8192 | tf_op jit(solution)/shard_map/all_to_all | solution.py:35
Sparse Core Ops, SparseCore 0:
  9.5 127.4 all-gather.1
where the time goes:
time: 366 us; the launch traced here: 363 us
  waiting for transfers between devices  212 us (58%)
  blocking collectives  58.2 us (16%)
  starting transfers between devices  31.5 us (9%)
  local copies, waits for them, and re-layouts  22.3 us (6%)
  matrix products  14.6 us (4%)
  between operations  13.8 us (4%)
  other arithmetic  10.9 us (3%)
    all_gather x1, waiting for transfers between devices, rows_first(): result = lax.all_gather(both, axis, axis=0, tiled=True)  91.5 us
    all_to_all x6, waiting for transfers between devices, copy_for_each(): return lax.all_to_all(copies, axis, split_axis=0, concat_axis=0, tiled=True)  91.1 us
    all_to_all x2, blocking collectives, sent_and_summed(): tiles = lax.all_to_all(in_blocks(array, dim, size), axis, 0, 0, tiled=True)  58.2 us
    all_to_all x1, waiting for transfers between devices, sent_and_summed(): tiles = lax.all_to_all(in_blocks(array, dim, size), axis, 0, 0, tiled=True)  26.8 us
    all_to_all x6, starting transfers between devices, copy_for_each(): return lax.all_to_all(copies, axis, split_axis=0, concat_axis=0, tiled=True)  22.3 us
    dot_general x3, matrix products, per_device(): jnp.dot(mixed, gathered_out[layer], preferred_element_type=jnp.float32)  9.02 us
    split x1, local copies, waits for them, and re-layouts, rows_first(): jnp.split(result, [sum(widths[:k]) for k in range(1, len(widths))], axis=1)  8.43 us
  transfers between devices with their start and end apart: 11, of which 11 were waited for; matrix products, arithmetic and copies ran while one was open for 1% of the time, Pallas kernels for 0%

commit v1 on v0

v1 whole, which is shorter than its diff:
```python
import functools

import jax
import jax.numpy as jnp
from jax import lax
from jax.experimental import pallas as pl
from jax.experimental.pallas import tpu as pltpu
from jax.sharding import PartitionSpec as P

EPS = 1e-06
HALO = 16
LANES = 128
CHUNK = 32
MESH = pl.DeviceIdType.MESH
F32 = jnp.float32
BF16 = jnp.bfloat16

A = [[(1, j), (2, j)] for j in range(8)]
B = [[(3, j), (4, j)] for j in range(8)]
C = [[(5, j)] for j in range(8)]
PLACES = {
    "start": [[(0, j)] for j in range(5)]
    + [[(0, 5)] + A[0], [(0, 6)] + A[1], [(0, 7)] + A[2]],
    ("halo", 0): A[3:4],
    ("mix", 0): A[4:8],
    ("square", 0): B[0:1],
    ("sum", 1): B[1:4],
    ("halo", 1): [B[4] + C[0]],
    ("mix", 1): [B[5] + C[1], B[6] + C[2], B[7] + C[3]],
    ("square", 1): C[4:5],
    ("sum", 2): C[5:7],
    ("halo", 2): C[7:8],
    ("mix", 2): [],
}


def kernel(
    n_sp, n_tp,
    stream, gain_pre, w_in, w_pool, pool_scale, w_out, gain_post, out,
    full, lhs0, win0, win, wout, lhs, cur, branch, own_y, rs_out, rs_in, mix, rows_acc,
    ss_out, ss_in, edge_out, edge_in, ext,
    ring_recv, part_recv, ring_send, swap_send, swap_recv, local_sem,
    x_send, x_recv, rs_send, rs_recv, ss_send, ss_recv, mix_send, mix_recv, edge_send, edge_recv,
):
    s = lax.axis_index("sp")
    t = lax.axis_index("tp")
    layers = w_in.shape[0]
    depth = w_in.shape[1]
    group = w_in.shape[2]
    tok, block = stream.shape
    width = gain_pre.shape[1]
    half = tok // 2
    chips = n_sp // 2
    plus = chips // 2
    minus = chips - 1 - plus
    span = n_sp // n_tp
    mats = 2 * layers
    quarter, rest = lax.div(s, span), lax.rem(s, span)
    home = {"sp": t * span + rest, "tp": quarter}
    stays = quarter == t
    moves = quarter != t
    up = {"sp": lax.rem(s + 2, n_sp)}
    down = {"sp": lax.rem(s + n_sp - 2, n_sp)}
    partner = {"sp": s + 1 - 2 * lax.rem(s, 2)}
    after = {"sp": lax.rem(s + 1, n_sp)}
    before = {"sp": lax.rem(s + n_sp - 1, n_sp)}
    tps = [lax.rem(t + k, n_tp) for k in range(n_tp)]

    def remote(src, dst, send, recv, device):
        copy = pltpu.make_async_remote_copy(
            src_ref=src, dst_ref=dst, send_sem=send, recv_sem=recv,
            device_id=device, device_id_type=MESH,
        )
        copy.start()
        return copy

    def arrived(ref, sem):
        pltpu.make_async_copy(ref, ref, sem).wait()

    barrier = pltpu.get_barrier_semaphore()
    greeted = [up, down, before, after] + [{"tp": k} for k in tps[1:]]
    for device in greeted:
        pl.semaphore_signal(barrier, inc=1, device_id=device, device_id_type=MESH)

    @pl.when(moves)
    def _():
        pl.semaphore_signal(barrier, inc=1, device_id=home, device_id_type=MESH)

    pl.semaphore_wait(barrier, len(greeted) + jnp.where(moves, 1, 0))

    def slot(m, src):
        if m % 2 == 0:
            rows = pl.ds(pl.multiple_of(src * depth, depth), depth)
            return win0.at[rows] if m == 0 else win.at[m // 2 - 1, rows]
        rows = pl.ds(pl.multiple_of(lax.div(src, span) * group, group), group)
        columns = pl.ds(pl.multiple_of(lax.rem(src, span) * depth, depth), depth)
        return wout.at[m // 2, rows, columns]

    def pieces(m, count):
        if m % 2 == 0:
            rows = pl.ds(0, count * depth)
            return win0.at[rows] if m == 0 else win.at[m // 2 - 1, rows]
        unit = group * depth // block
        return wout.at[m // 2, pl.ds(0, count * unit)]

    def original(m):
        return w_in.at[m // 2] if m % 2 == 0 else w_out.at[m // 2]

    def spread_own(m):
        src = slot(m, s) if m else original(0)
        remote(src, slot(m, s), ring_send.at[m], ring_recv.at[m, 0, 0], up)
        remote(src, slot(m, s), ring_send.at[m], ring_recv.at[m, 1, 0], down)
        remote(src, slot(m, s), ring_send.at[m], part_recv.at[m], partner)

    def swap_started(m):
        here = home["sp"]

        @pl.when(moves)
        def _():
            remote(original(m), slot(m, s_of_home(m)), swap_send.at[m], swap_recv.at[m], home)

        @pl.when(stays)
        def _():
            pltpu.make_async_copy(original(m), slot(m, s), swap_recv.at[m]).start()

    def s_of_home(m):
        return home["sp"]

    def swap_ended(m):
        arrived(slot(m, s), swap_recv.at[m])

    def step(m, j):
        if j == 0 and m > 0:
            swap_ended(m)
            spread_own(m)
        for way, reach, device in ((0, plus, up), (1, minus, down)):
            if j >= reach:
                continue
            distance = 2 * (j + 1)
            src = lax.rem(s + n_sp - distance if way == 0 else s + distance, n_sp)
            piece = slot(m, src)
            arrived(piece, ring_recv.at[m, way, j])
            if j + 1 < reach:
                remote(piece, piece, ring_send.at[m], ring_recv.at[m, way, j + 1], device)
            remote(piece, piece, ring_send.at[m], part_recv.at[m], partner)

    def ticks(place):
        for tick in PLACES.get(place, []):
            for m, j in tick:
                step(m, j)

    def whole(m):
        arrived(pieces(m, chips), part_recv.at[m])

    lo, hi = pl.ds(0, half), pl.ds(half, half)
    spread_own(0)
    mine = full.at[t]
    right, left = {"tp": tps[1]}, {"tp": tps[n_tp - 1]}
    remote(stream.at[lo], mine.at[lo], x_send.at[0], x_recv.at[0], right)
    remote(stream.at[hi], mine.at[hi], x_send.at[1], x_recv.at[1], left)
    swap_started(1)
    remote(stream.at[hi], mine.at[hi], x_send.at[2], x_recv.at[2], right)
    remote(stream.at[lo], mine.at[lo], x_send.at[3], x_recv.at[3], left)
    own_rows = pltpu.make_async_copy(stream, mine, local_sem.at[0])
    own_rows.start()
    own_piece = pltpu.make_async_copy(original(0), slot(0, s), local_sem.at[1])
    own_piece.start()
    for m in range(2, mats):
        swap_started(m)

    def squares(x):
        total = x[:, :LANES] * x[:, :LANES]
        for k in range(1, x.shape[1] // LANES):
            part = x[:, k * LANES:(k + 1) * LANES]
            total = total + part * part
        return total

    def prepare(b, first):
        gain = gain_pre[0:1, pl.ds(pl.multiple_of(b * block, block), block)]

        @pl.loop(0, tok // CHUNK)
        def _(i):
            rows = pl.ds(pl.multiple_of(i * CHUNK, CHUNK), CHUNK)
            x = full[b, rows, :].astype(F32)
            lhs0[b, rows, :] = (x * gain).astype(BF16)
            sums = squares(x)
            rows_acc[rows, :] = sums if first else rows_acc[rows, :] + sums

    start = PLACES["start"]

    def start_tick(i):
        for m, j in start[i]:
            step(m, j)

    start_tick(0)
    own_rows.wait()
    prepare(t, True)
    start_tick(1)
    behind, ahead, across = full.at[tps[n_tp - 1]], full.at[tps[1]], full.at[tps[2]]
    arrived(behind.at[lo], x_recv.at[0])
    remote(behind.at[lo], behind.at[lo], x_send.at[4], x_recv.at[4], right)
    arrived(ahead.at[hi], x_recv.at[1])
    remote(ahead.at[hi], ahead.at[hi], x_send.at[5], x_recv.at[5], left)
    start_tick(2)
    start_tick(3)
    arrived(behind.at[hi], x_recv.at[2])
    arrived(ahead.at[lo], x_recv.at[3])
    prepare(tps[n_tp - 1], False)
    start_tick(4)
    prepare(tps[1], False)
    start_tick(5)
    arrived(across.at[lo], x_recv.at[4])
    arrived(across.at[hi], x_recv.at[5])
    start_tick(6)
    prepare(tps[2], False)
    start_tick(7)
    own_piece.wait()
    whole(0)

    def row_of(acc):
        return jnp.broadcast_to(jnp.sum(acc.T, axis=0, keepdims=True), (8, tok))

    def inverse(row):
        inv = lax.rsqrt(row / width + EPS)
        return jnp.concatenate([inv] * (LANES // 8), axis=0).T

    def across_lanes(column, lanes):
        return jnp.concatenate([column] * (lanes // LANES), axis=1)

    def send_squares(kind, row):
        ss_out[kind] = row
        for k in range(1, n_tp):
            remote(
                ss_out.at[kind], ss_in.at[kind, k], ss_send.at[kind, k], ss_recv.at[kind, k],
                {"tp": tps[k]},
            )

    def sum_squares(kind):
        total = ss_out[kind]
        for k in range(1, n_tp):
            arrived(ss_in.at[kind, k], ss_recv.at[kind, k])
            total = total + ss_in[kind, k]
        return total

    position = s * tok + lax.broadcasted_iota(jnp.int32, (tok, LANES), 0)
    window = 2
    for k in range(1, n_tp):
        window = jnp.where(t == k, 2 << k, window)
    count = jnp.minimum(position + 1, window).astype(F32)

    for l in range(layers):
        if l == 0:
            acc = jnp.dot(lhs0[0], win0[0:block, :], preferred_element_type=F32)
            for b in range(1, n_tp):
                acc = acc + jnp.dot(
                    lhs0[b], win0[b * block:(b + 1) * block, :], preferred_element_type=F32
                )
            inv = inverse(row_of(rows_acc[...]))
        else:
            whole(2 * l)
            for k in (2, 1, 3, 0):
                first = pl.multiple_of(tps[k] * block, block)
                y = jnp.dot(lhs[...], win[l - 1, pl.ds(first, block), :], preferred_element_type=F32)
                if k == 0:
                    own_y[...] = y
                else:
                    rs_out[l - 1, k] = y.astype(BF16)
                    remote(
                        rs_out.at[l - 1, k], rs_in.at[l - 1, k],
                        rs_send.at[l - 1, k], rs_recv.at[l - 1, k], {"tp": tps[k]},
                    )
            ticks(("sum", l))
            inv = inverse(sum_squares(layers + l - 1))
            acc = own_y[...]
            for k in range(1, n_tp):
                arrived(rs_in.at[l - 1, k], rs_recv.at[l - 1, k])
                acc = acc + rs_in[l - 1, k].astype(F32)
        inner = (acc * across_lanes(inv, group)).astype(BF16)
        edge_out[l] = inner[tok - HALO:, :]
        remote(edge_out.at[l], edge_in.at[l], edge_send.at[l], edge_recv.at[l], after)
        inner = inner.astype(F32)
        ext[HALO:, :] = inner
        ticks(("halo", l))
        arrived(edge_in.at[l], edge_recv.at[l])
        ext[0:HALO, :] = jnp.where(s > 0, edge_in[l].astype(F32), 0.0)
        sums = ext[...]
        chosen = None
        for k in range(n_tp):
            sums = sums + pltpu.roll(sums, 1 << k, 0)
            chosen = sums if chosen is None else jnp.where(t >= k, sums, chosen)
        pooled = chosen[HALO:, :] / across_lanes(count, group)
        spread = (pooled - ext[HALO:, :]).astype(BF16)
        mixed = jnp.dot(spread, w_pool[l, 0], preferred_element_type=F32)
        mixed = (mixed * pool_scale[l:l + 1, :]).astype(BF16)
        own = pl.ds(pl.multiple_of(t * group, group), group)
        mix[l, :, own] = mixed
        place = mix.at[l, :, own]
        for k in (2, 1, 3):
            remote(place, place, mix_send.at[l, k], mix_recv.at[l, k], {"tp": tps[k]})
        ticks(("mix", l))
        for k in (1, 3, 2):
            theirs = pl.ds(pl.multiple_of(tps[(n_tp - k) % n_tp] * group, group), group)
            arrived(mix.at[l, :, theirs], mix_recv.at[l, k])
        whole(2 * l + 1)
        total = None
        for n in range(block // group):
            columns = slice(n * group, (n + 1) * group)
            y = jnp.dot(mix[l], wout[l, :, columns], preferred_element_type=F32)
            branch[:, columns] = y
            total = squares(y) if total is None else total + squares(y)
        send_squares(l, row_of(total))
        ticks(("square", l))
        rows_acc[...] = inverse(sum_squares(l))
        mine_only = pl.ds(pl.multiple_of(t * block, block), block)
        gain = gain_post[l:l + 1, mine_only]
        before_l = full.at[t] if l == 0 else cur
        if l + 1 < layers:
            next_gain = gain_pre[l + 1:l + 2, mine_only]

        @pl.loop(0, tok // CHUNK)
        def _(i):
            rows = pl.ds(pl.multiple_of(i * CHUNK, CHUNK), CHUNK)
            scale = across_lanes(rows_acc[rows, :], block)
            new = before_l[rows, :].astype(F32) + branch[rows, :] * scale * gain
            new = new.astype(BF16)
            if l + 1 < layers:
                cur[rows, :] = new
                new = new.astype(F32)
                lhs[rows, :] = (new * next_gain).astype(BF16)
                rows_acc[rows, :] = squares(new)
            else:
                out[rows, :] = new

        if l + 1 < layers:
            send_squares(layers + l, row_of(rows_acc[...]))

    for m in range(mats):
        arrived(pieces(m, plus + minus + chips), ring_send.at[m])
        if m:
            @pl.when(moves)
            def _():
                arrived(slot(m, s), swap_send.at[m])
    for k in range(6):
        arrived(mine.at[lo], x_send.at[k])
    for l in range(layers):
        arrived(edge_out.at[l], edge_send.at[l])
        for k in range(1, n_tp):
            arrived(mix.at[l, :, pl.ds(0, group)], mix_send.at[l, k])
            arrived(ss_out.at[l], ss_send.at[l, k])
            if l:
                arrived(rs_out.at[l - 1, k], rs_send.at[l - 1, k])
                arrived(ss_out.at[l], ss_send.at[layers + l - 1, k])


def solution(mesh):
    n_sp, n_tp = mesh.shape["sp"], mesh.shape["tp"]

    def per_device(stream, gain_pre, w_in, w_pool, pool_scale, w_out, gain_post):
        tok, block = stream.shape
        layers, depth, group = w_in.shape
        width = gain_pre.shape[1]
        channels = n_tp * group
        mats = 2 * layers
        kinds = 2 * layers - 1
        reach = n_sp // 4
        dma = pltpu.SemaphoreType.DMA
        vmem = pl.BlockSpec(memory_space=pltpu.VMEM)
        hbm = pl.BlockSpec(memory_space=pl.ANY)
        return pl.pallas_call(
            functools.partial(kernel, n_sp, n_tp),
            out_shape=jax.ShapeDtypeStruct((tok, block), BF16),
            in_specs=[hbm, vmem, hbm, vmem, vmem, hbm, vmem],
            out_specs=vmem,
            scratch_shapes=[
                pltpu.VMEM((n_tp, tok, block), BF16),
                pltpu.VMEM((n_tp, tok, block), BF16),
                pltpu.VMEM((width, group), BF16),
                pltpu.VMEM((layers - 1, n_tp * block, group), BF16),
                pltpu.VMEM((layers, channels, block), BF16),
                pltpu.VMEM((tok, block), BF16),
                pltpu.VMEM((tok, block), BF16),
                pltpu.VMEM((tok, block), F32),
                pltpu.VMEM((tok, group), F32),
                pltpu.VMEM((layers - 1, n_tp, tok, group), BF16),
                pltpu.VMEM((layers - 1, n_tp, tok, group), BF16),
                pltpu.VMEM((layers, tok, channels), BF16),
                pltpu.VMEM((tok, LANES), F32),
                pltpu.VMEM((kinds, 8, tok), F32),
                pltpu.VMEM((kinds, n_tp, 8, tok), F32),
                pltpu.VMEM((layers, HALO, group), BF16),
                pltpu.VMEM((layers, HALO, group), BF16),
                pltpu.VMEM((HALO + tok, group), F32),
                dma((mats, 2, reach)),
                dma((mats,)),
                dma((mats,)),
                dma((mats,)),
                dma((mats,)),
                dma((2,)),
                dma((6,)),
                dma((6,)),
                dma((layers - 1, n_tp)),
                dma((layers - 1, n_tp)),
                dma((kinds, n_tp)),
                dma((kinds, n_tp)),
                dma((layers, n_tp)),
                dma((layers, n_tp)),
                dma((layers,)),
                dma((layers,)),
            ],
            compiler_params=pltpu.CompilerParams(
                collective_id=0, has_side_effects=True, vmem_limit_bytes=60 * 1024 * 1024
            ),
        )(stream, gain_pre, w_in, w_pool, pool_scale, w_out, gain_post)

    return jax.shard_map(
        per_device,
        mesh=mesh,
        in_specs=(
            P(("grp", "sp"), "tp"),
            P(),
            P(None, "sp", "tp"),
            P(None, "tp", None, None),
            P(None, "tp"),
            P(None, "tp", "sp"),
            P(),
        ),
        out_specs=P(("grp", "sp"), "tp"),
        check_vma=False,
    )
```

time: 366 us -> 196 us (0.54)
  waiting for transfers between devices: 212 us -> 0 us
  Pallas kernels: 0 us -> 194 us
  blocking collectives: 58.2 us -> 0 us
  starting transfers between devices: 31.5 us -> 0 us
  local copies, waits for them, and re-layouts: 22.3 us -> 1.87 us
  matrix products: 14.6 us -> 0 us
  between operations: 13.8 us -> 0.01 us
  other arithmetic: 10.9 us -> 0 us
    pallas_call x0 -> x1, Pallas kernels: none -> 194 us  [per_device(): pl.pallas_call(functools.partial(kernel, n_sp, n_tp), out_shape=jax.Shape...]
    all_to_all x7 -> x0, waiting for transfers between devices: 118 us -> none  [the longest x6 91.1 us: copy_for_each(): return lax.all_to_all(copies, axis, split_axis=0, concat_axis=0, tiled=True)]
    all_gather x1 -> x0, waiting for transfers between devices: 91.5 us -> none  [rows_first(): result = lax.all_gather(both, axis, axis=0, tiled=True)]
    all_to_all x2 -> x0, blocking collectives: 58.2 us -> none  [sent_and_summed(): tiles = lax.all_to_all(in_blocks(array, dim, size), axis, 0, 0, tiled=True)]
    all_to_all x7 -> x0, starting transfers between devices: 26.7 us -> none  [the longest x6 22.3 us: copy_for_each(): return lax.all_to_all(copies, axis, split_axis=0, concat_axis=0, tiled=True)]
    dot_general x6 -> x0, matrix products: 14.6 us -> none  [the longest x3 9.02 us: per_device(): jnp.dot(mixed, gathered_out[layer], preferred_element_type=jnp.float32)]
    split x1 -> x0, local copies, waits for them, and re-layouts: 8.43 us -> none  [rows_first(): jnp.split(result, [sum(widths[:k]) for k in range(1, len(widths))], axis=1)]
    broadcast_in_dim x6 -> x0, local copies, waits for them, and re-layouts: 6.26 us -> none  [copy_for_each(): copies = jnp.broadcast_to(array, (lax.axis_size(axis), *array.shape))]
  transfers between devices with their start and end apart: 11 -> 0, of which waited for: 11 -> 0; matrix products, arithmetic and copies ran while one was open for 1% -> 0% of each run, Pallas kernels for 0% -> 0%
where the time goes in v1:
time: 196 us
  Pallas kernels  194 us (99%)
    pallas_call x1, Pallas kernels, per_device(): pl.pallas_call(functools.partial(kernel, n_sp, n_tp), out_shape=jax.Shape...  194 us

profile of v1, /device:TPU:40, one launch (start us, length us, event | category | flops | bytes accessed | tf_op | source)
XLA Modules:
  0.0 195.7 jit_solution(12191906906778563409)
XLA Ops:
  0.0 193.9 %shard_map.73 = bf16[256,1024]{1,0:T(8,128)(2,1)} custom-call(bf16[256,1024]{1,0:T(8,128)(2,1)} %stream.1, f32[3,4096]{1,0:T(4,128)} %gain_pre.1, bf16[3,128,256]{2,1,0:T(8,128)(2,1)} %w_in.1, bf16[3,1,256,256]{3,2,1,0:T(8,128)(2,1)} %w_pool.1, f32[3,256]{1,0:T(4,128)} %pool_scale.1, bf16[3,256,128]{2,1,0:T(8,128)(2,1)} %w_out.1, f32[3,4096]{1,0:T(4,128)} %gain_post.1), custom_call_target="tpu_custom_call" | custom-call | tf_op jit(solution)/shard_map/pallas_call | solution.py:369
  193.9 1.9 copy.9
